TPU v7x, 32 devices: a whole 2x2x4 slice. The times are simulated.
32 devices in a mesh: kv: 16 (over z, y, x), tp: 2 (over core).
Axes of the slice: x: 2, y: 2, z: 4, core: 2. Of those that a mesh axis runs over, the one named last changes fastest.
Arguments:
- tokens: bfloat16 [160, 3, 2048], P('kv', None, 'tp'), may hold values from -6 to 6
- norm_gain: float32 [2048], replicated, may hold values from 0.1 to 1.9
- w_query: bfloat16 [2048, 1024], P('kv', 'tp'), may hold values from -0.125 to 0.125
- w_key: bfloat16 [2048, 1024], P('kv', 'tp'), may hold values from -0.125 to 0.125
- w_value: bfloat16 [2048, 2048], P('kv', 'tp'), may hold values from -0.125 to 0.125
- w_igate: bfloat16 [2048, 8], replicated, may hold values from -0.125 to 0.125
- w_fgate: bfloat16 [2048, 8], replicated, may hold values from -0.125 to 0.125
- igate_bias: float32 [8], replicated, may hold values from -5 to -2
- fgate_bias: float32 [8], replicated, may hold values from 0.5 to 4
- prev_keys: bfloat16 [160, 3, 1024], P('kv', None, 'tp'), may hold values from -6 to 6
- prev_values: bfloat16 [160, 3, 2048], P('kv', None, 'tp'), may hold values from -6 to 6
- prev_igate: float32 [160, 3, 8], P('kv', None, 'tp'), may hold values from -4 to 0
- prev_logf: float32 [160, 3, 8], P('kv', None, 'tp'), may hold values from -0.6 to -0.02
- accepted: int32 [160], P('kv'), may hold values from 0 to 3
- state_mem: float32 [160, 8, 128, 256], P('kv', 'tp'), may hold values from -2 to 2
- state_norm: float32 [160, 8, 128], P('kv', 'tp'), may hold values from -2 to 2
- state_max: float32 [160, 8], P('kv', 'tp'), may hold values from -3 to 0
Outputs:
- readout: bfloat16 [160, 3, 2048], P('kv', None, 'tp')
- base_mem: float32 [160, 8, 128, 256], P('kv', 'tp')
- base_norm: float32 [160, 8, 128], P('kv', 'tp')
- base_max: float32 [160, 8], P('kv', 'tp')
Inputs may be any that keep to these rules, and one draw needn't show every extreme that they name: Proposal j of a sequence is live when j < accepted of that sequence.
All inputs are finite; a program needn't handle non-finite values.
Results may differ from a plain program's by a relative error of at most 0.0073.
Values may be sent and summed in bfloat16 or wider, within the bound.
No kernel may reach another device: no remote copies, remote signals or barrier semaphores. Data moves between devices by JAX's collectives and lax.ppermute only.
A program may use at most 64 MiB of HBM per device.

v0:
```python
import jax
import jax.numpy as jnp
from jax import lax
from jax.sharding import PartitionSpec as P

epsilon = 1e-06
highest = lax.Precision.HIGHEST


def fold_accepted(
    state_mem, state_norm, state_max, key_rows, value_rows, in_gate, log_forget, accepted
):
    length = key_rows.shape[1]
    live_mask = (jnp.arange(length, dtype=jnp.int32)[None, :] < accepted[:, None])[:, :, None]
    forget_live = jnp.where(live_mask, log_forget, 0.0)
    cumulative = jnp.cumsum(forget_live, axis=1)
    totals = cumulative[:, -1]
    weight_log = jnp.where(live_mask, totals[:, None] - cumulative + in_gate, -jnp.inf)
    base_max = jnp.maximum(totals + state_max, jnp.max(weight_log, axis=1))
    carry_weight = jnp.exp(totals + state_max - base_max)
    weights = jnp.exp(weight_log - base_max[:, None])
    base_mem = carry_weight[..., None, None] * state_mem + jnp.einsum(
        "sph,sphd,sphv->shdv", weights, key_rows, value_rows, precision=highest
    )
    base_norm = carry_weight[..., None] * state_norm + jnp.einsum(
        "sph,sphd->shd", weights, key_rows, precision=highest
    )
    return (base_mem, base_norm, base_max)


def readout_block(
    base_mem, base_norm, base_max, query_rows, key_rows, value_rows, in_gate, log_forget
):
    length = query_rows.shape[1]
    cumulative = jnp.cumsum(log_forget, axis=1)
    causal = (
        jnp.arange(length, dtype=jnp.int32)[:, None] >= jnp.arange(length, dtype=jnp.int32)[None, :]
    )
    within_log = cumulative[:, :, None, :] - cumulative[:, None, :, :] + in_gate[:, None, :, :]
    within_log = jnp.where(causal[None, :, :, None], within_log, -jnp.inf)
    carried_log = cumulative + base_max[:, None, :]
    top_log = jnp.maximum(carried_log, jnp.max(within_log, axis=2))
    scores = jnp.einsum("sthd,suhd->stuh", query_rows, key_rows, precision=highest) * jnp.exp(
        within_log - top_log[:, :, None, :]
    )
    carried_weight = jnp.exp(carried_log - top_log)
    numerator = jnp.einsum(
        "stuh,suhv->sthv", scores, value_rows, precision=highest
    ) + carried_weight[..., None] * jnp.einsum(
        "sthd,shdv->sthv", query_rows, base_mem, precision=highest
    )
    denominator = jnp.sum(scores, axis=2) + carried_weight * jnp.einsum(
        "sthd,shd->sth", query_rows, base_norm, precision=highest
    )
    return numerator / jnp.maximum(jnp.abs(denominator), jnp.exp(-top_log))[..., None]


def shards(
    tokens,
    norm_gain,
    w_query,
    w_key,
    w_value,
    w_igate,
    w_fgate,
    igate_bias,
    fgate_bias,
    prev_keys,
    prev_values,
    prev_igate,
    prev_logf,
    accepted,
    state_mem,
    state_norm,
    state_max,
):
    seq_count, length, part_width = tokens.shape
    head_count = state_mem.shape[1]
    key_width = state_mem.shape[2]
    value_width = state_mem.shape[3]
    key_scale = key_width ** (-0.5)
    row_count = seq_count * length
    gathered = lax.all_gather(tokens.reshape(row_count, part_width), "tp", axis=1, tiled=True)
    flattened = gathered.astype(jnp.float32)
    normed = (
        flattened
        * lax.rsqrt(jnp.mean(flattened * flattened, axis=-1, keepdims=True) + epsilon)
        * norm_gain
    ).astype(jnp.bfloat16)
    stacked = jnp.concatenate([w_query, w_key, w_value], axis=1)
    spread = lax.all_to_all(normed, "kv", split_axis=1, concat_axis=0, tiled=True)
    projected = lax.psum_scatter(
        jnp.dot(spread, stacked, preferred_element_type=jnp.float32),
        "kv",
        scatter_dimension=0,
        tiled=True,
    )
    query_cols = head_count * key_width
    query_rows = projected[:, :query_cols].astype(jnp.bfloat16)
    key_rows = projected[:, query_cols : 2 * query_cols].astype(jnp.bfloat16)
    value_rows = projected[:, 2 * query_cols :].astype(jnp.bfloat16)
    head_start = lax.axis_index("tp") * head_count
    input_weight = lax.dynamic_slice_in_dim(w_igate, head_start, head_count, 1)
    forget_weight = lax.dynamic_slice_in_dim(w_fgate, head_start, head_count, 1)
    in_gate = jnp.dot(
        normed, input_weight, preferred_element_type=jnp.float32
    ) + lax.dynamic_slice_in_dim(igate_bias, head_start, head_count, 0)
    log_forget = jax.nn.log_sigmoid(
        jnp.dot(normed, forget_weight, preferred_element_type=jnp.float32)
        + lax.dynamic_slice_in_dim(fgate_bias, head_start, head_count, 0)
    )

    def split_heads(matrix, last_width):
        return matrix.astype(jnp.float32).reshape(seq_count, length, head_count, last_width)

    base_mem, base_norm, base_max = fold_accepted(
        state_mem,
        state_norm,
        state_max,
        split_heads(prev_keys, key_width) * key_scale,
        split_heads(prev_values, value_width),
        prev_igate,
        prev_logf,
        accepted,
    )
    hidden = readout_block(
        base_mem,
        base_norm,
        base_max,
        split_heads(query_rows, key_width),
        split_heads(key_rows, key_width) * key_scale,
        split_heads(value_rows, value_width),
        in_gate.reshape(seq_count, length, head_count),
        log_forget.reshape(seq_count, length, head_count),
    )
    readout = hidden.reshape(seq_count, length, head_count * value_width).astype(jnp.bfloat16)
    return (readout, base_mem, base_norm, base_max)


def solution(mesh):
    return jax.shard_map(
        shards,
        mesh=mesh,
        in_specs=(
            P("kv", None, "tp"),
            P(),
            P("kv", "tp"),
            P("kv", "tp"),
            P("kv", "tp"),
            P(),
            P(),
            P(),
            P(),
            P("kv", None, "tp"),
            P("kv", None, "tp"),
            P("kv", None, "tp"),
            P("kv", None, "tp"),
            P("kv"),
            P("kv", "tp", None, None),
            P("kv", "tp", None),
            P("kv", "tp"),
        ),
        out_specs=(
            P("kv", None, "tp"),
            P("kv", "tp", None, None),
            P("kv", "tp", None),
            P("kv", "tp"),
        ),
        check_vma=False,
    )
```

profile of v0, /device:TPU:16, one launch (start us, length us, event | category | flops | bytes accessed | tf_op | source)
XLA Modules:
  0.0 143.2 jit_solution(959274244908550986)
XLA Ops:
  0.6 1.0 reshape.103
  1.6 1.9 %all_gather.3 = bf16[30,2048]{1,0:T(8,128)(2,1)S(1)} all-gather(bf16[30,1024]{1,0:T(8,128)(2,1)S(1)} %reshape.103), channel_id=1, replica_groups=mesh['kv'=16,'tp'=2] {'tp'}, dimensions={1}, use_global_device_ids=true | all-gather | bytes 184320 | tf_op jit(solution)/shard_map/all_gather | solution.py:83
  3.5 0.1 fusion.13
  3.7 0.8 fusion.15
  4.5 0.7 copy.114
  5.2 7.1 %all-to-all-start = ((bf16[30,16,128]{2,0,1:T(8,128)(2,1)}), bf16[30,16,128]{2,0,1:T(8,128)(2,1)S(1)}, u32[]{:S(2)}, u32[]{:S(2)}) async-start(bf16[30,16,128]{2,0,1:T(8,128)(2,1)} %copy.114), calls=%async_computation | async-start | bytes 262144 | tf_op jit(solution)/shard_map/all_to_all | solution.py:91
  12.3 0.7 iota_compare_fusion
  13.0 0.7 dynamic_slice.15
  13.7 0.7 dynamic_slice.13
  14.4 0.7 fusion.31
  15.2 0.7 fusion.44
  16.0 0.8 copy.122
  16.9 0.8 reshape.111
  17.7 0.9 fusion.37
  18.8 0.1 copy.117
  18.9 0.1 copy.118
  19.0 0.9 convolution_add_fusion
  20.0 0.2 fusion.19
  20.6 8.0 %multiply_add_fusion = f32[10,4,128,256]{3,2,1,0:T(8,128)} fusion(f32[10,4,128,256]{3,2,1,0:T(8,128)} %param.31, f32[10,4]{1,0:T(8,128)S(1)} %get-tuple-element.14, bf16[10,3,4,256]{3,1,2,0:T(4,128)(2,1)S(1)} %bitcast.57, f32[10,3,4,128]{3,2,1,0:T(4,128)S(1)} %get-tuple-element.19), kind=kOutput, calls=%fused_computation | convolution fusion | flops 49807360 | bytes 10608800 | tf_op jit(solution)/shard_map/sph,sphd,sphv->shdv/dot_general | solution.py:22
  28.6 0.1 copy.138
  28.8 0.6 dynamic-slice.4
  30.0 0.4 fusion.20
  30.5 2.5 %fusion.7 = f32[480,2048]{1,0:T(8,128)} fusion(bf16[480,128]{1,0:T(8,128)(2,1)S(1)} %all_to_all.17, bf16[128,1024]{1,0:T(8,128)(2,1)S(1)} %copy-done.1, bf16[128,512]{1,0:T(8,128)(2,1)S(1)} %copy-done.2, bf16[128,512]{1,0:T(8,128)(2,1)S(1)} %copy-done.3), kind=kOutput, calls=%fused_computation.12 | convolution fusion | flops 253231104 | bytes 4579328 | tf_op jit(solution)/shard_map/dot_general | solution.py:93
  33.1 94.6 %fusion = f32[32,2048]{1,0:T(8,128)S(1)} fusion(f32[480,2048]{1,0:T(8,128)} %fusion.7), kind=kCustom, calls=%all-reduce-scatter | all-reduce-scatter fusion | flops 1048577 | bytes 4194816
  127.8 1.9 %collective-permute-start = (bf16[30,2048]{1,0:T(8,128)(2,1)S(1)}, bf16[30,2048]{1,0:T(8,128)(2,1)S(1)}, u32[]{:S(2)}, u32[]{:S(2)}) collective-permute-start(bf16[30,2048]{1,0:T(8,128)(2,1)S(1)} %slice.23), channel_id=1, source_target_pairs={{0,2},{2,4},{4,6},{6,8},{8,10},{10,12},{12,14},{14,16},{16,18},{18... | collective-permute-start | bytes 368648
  129.8 6.7 %collective-permute-done = bf16[30,2048]{1,0:T(8,128)(2,1)S(1)} collective-permute-done((bf16[30,2048]{1,0:T(8,128)(2,1)S(1)}, bf16[30,2048]{1,0:T(8,128)(2,1)S(1)}, u32[]{:S(2)}, u32[]{:S(2)}) %collective-permute-start) | collective-permute-done | bytes 122912
  136.5 0.3 concatenate.4
  136.8 0.3 fusion.23
  137.3 0.3 fusion.45
  137.8 0.1 copy.135
  138.0 4.2 %fusion.3 = f32[10,3,4,256]{3,1,2,0:T(4,128)S(1)} fusion(f32[10,4,128,256]{3,2,1,0:T(8,128)} %multiply_add_fusion, f32[10,3,4]{1,2,0:T(4,128)S(1)} %copy.129, bf16[10,3,4,128]{3,2,1,0:T(4,128)(2,1)S(1)} %reshape.105), kind=kOutput, calls=%fused_computation.5 | convolution fusion | flops 47216640 | bytes 5396960 | tf_op jit(solution)/shard_map/sthd,shdv->sthv/dot_general | solution.py:49
  142.2 1.0 fusion.4
  (49 shorter events, 1.7 us)
Async XLA Ops:
  0.6 19.9 %copy-start = (bf16[10,3,1024]{2,1,0:T(4,128)(2,1)S(1)}, bf16[10,3,1024]{2,1,0:T(4,128)(2,1)}, u32[]{:S(2)}) copy-start(bf16[10,3,1024]{2,1,0:T(4,128)(2,1)} %param.27) | copy-start | bytes 184324
  5.2 25.2 %all-to-all-start = ((bf16[30,16,128]{2,0,1:T(8,128)(2,1)}), bf16[30,16,128]{2,0,1:T(8,128)(2,1)S(1)}, u32[]{:S(2)}, u32[]{:S(2)}) async-start(bf16[30,16,128]{2,0,1:T(8,128)(2,1)} %copy.114), calls=%async_computation | async-start | bytes 262144 | tf_op jit(solution)/shard_map/all_to_all | solution.py:91
  16.9 120.8 %copy-start.6 = (f32[10,4]{0,1:T(4,128)}, f32[10,4]{0,1:T(4,128)S(1)}, u32[]{:S(2)}) copy-start(f32[10,4]{0,1:T(4,128)S(1)} %copy.124) | copy-start | bytes 484
  20.6 8.2 %copy-start.7 = (u32[32]{0:T(128)S(1)}, u32[32]{0:T(128)}, u32[]{:S(2)}) copy-start(u32[32]{0:T(128)} %constant.39) | copy-start | bytes 388
  20.6 9.9 %copy-start.1 = (bf16[128,1024]{1,0:T(8,128)(2,1)S(1)}, bf16[128,1024]{1,0:T(8,128)(2,1)}, u32[]{:S(2)}) copy-start(bf16[128,1024]{1,0:T(8,128)(2,1)} %param.21) | copy-start | bytes 786436
  20.6 9.9 %copy-start.2 = (bf16[128,512]{1,0:T(8,128)(2,1)S(1)}, bf16[128,512]{1,0:T(8,128)(2,1)}, u32[]{:S(2)}) copy-start(bf16[128,512]{1,0:T(8,128)(2,1)} %param.20) | copy-start | bytes 393220
  20.6 9.9 %copy-start.3 = (bf16[128,512]{1,0:T(8,128)(2,1)S(1)}, bf16[128,512]{1,0:T(8,128)(2,1)}, u32[]{:S(2)}) copy-start(bf16[128,512]{1,0:T(8,128)(2,1)} %param.19) | copy-start | bytes 393220
  30.5 99.2 %copy-start.4 = (f32[10,4,128]{2,1,0:T(4,128)S(1)}, f32[10,4,128]{2,1,0:T(4,128)}, u32[]{:S(2)}) copy-start(f32[10,4,128]{2,1,0:T(4,128)} %param.32) | copy-start | bytes 61444
  127.8 8.7 %collective-permute-start = (bf16[30,2048]{1,0:T(8,128)(2,1)S(1)}, bf16[30,2048]{1,0:T(8,128)(2,1)S(1)}, u32[]{:S(2)}, u32[]{:S(2)}) collective-permute-start(bf16[30,2048]{1,0:T(8,128)(2,1)S(1)} %slice.23), channel_id=1, source_target_pairs={{0,2},{2,4},{4,6},{6,8},{8,10},{10,12},{12,14},{14,16},{16,18},{18... | collective-permute-start | bytes 368648
  129.8 13.4 %copy-start.5 = (f32[10,4,128]{2,1,0:T(4,128)}, f32[10,4,128]{2,1,0:T(4,128)S(1)}, u32[]{:S(2)}) copy-start(f32[10,4,128]{2,1,0:T(4,128)S(1)} %multiply_add_fusion.1) | copy-start | bytes 61444
where the time goes:
time: 144 us; the launch traced here: 143 us
  blocking collectives  96.5 us (67%)
  matrix products  18.6 us (13%)
  starting transfers between devices  9.03 us (6%)
  local copies, waits for them, and re-layouts  7.4 us (5%)
  waiting for transfers between devices  6.66 us (5%)
  other arithmetic  3.44 us (2%)
  between operations  1.6 us (1%)
    unnamed x1, blocking collectives  94.6 us
    dot_general x1, matrix products, fold_accepted(): jnp.einsum('sph,sphd,sphv->shdv', weights, key_rows, value_rows, precisio...  7.97 us
    all_to_all x1, starting transfers between devices, shards(): lax.all_to_all(normed, 'kv', split_axis=1, concat_axis=0, tiled=True)  7.11 us
    unnamed x1, waiting for transfers between devices  6.66 us
    dot_general x1, matrix products, readout_block(): jnp.einsum('sthd,shdv->sthv', query_rows, base_mem, precision=highest)  4.24 us
  transfers between devices with their start and end apart: 2, of which 1 were waited for; matrix products, arithmetic and copies ran while one was open for 12% of the time, Pallas kernels for 0%

commit v1 on v0

--- a/solution.py
+++ b/solution.py
@@ -88,7 +88,10 @@
         * norm_gain
     ).astype(jnp.bfloat16)
     stacked = jnp.concatenate([w_query, w_key, w_value], axis=1)
-    spread = lax.all_to_all(normed, "kv", split_axis=1, concat_axis=0, tiled=True)
+    spread = jnp.concatenate(
+        lax.all_to_all(jnp.stack(jnp.split(normed, lax.axis_size("kv"), axis=1)), "kv", 0, 0),
+        axis=0,
+    )
     projected = lax.psum_scatter(
         jnp.dot(spread, stacked, preferred_element_type=jnp.float32),
         "kv",

time: 144 us -> 153 us (1.062)
  local copies, waits for them, and re-layouts: 7.4 us -> 16.3 us
    unnamed x22 -> x36, local copies, waits for them, and re-layouts: 1.8 us -> 10.7 us
  transfers between devices with their start and end apart: 2 -> 2, of which waited for: 1 -> 1; matrix products, arithmetic and copies ran while one was open for 12% -> 11% of each run, Pallas kernels for 0% -> 0%
where the time goes in v1:
time: 153 us; the launch traced here: 152 us
  blocking collectives  96.5 us (63%)
  matrix products  18.6 us (12%)
  local copies, waits for them, and re-layouts  16.3 us (11%)
  starting transfers between devices  9.03 us (6%)
  waiting for transfers between devices  6.65 us (4%)
  other arithmetic  3.44 us (2%)
  between operations  1.59 us (1%)
    unnamed x1, blocking collectives  94.6 us
    unnamed x36, local copies, waits for them, and re-layouts  10.7 us
    dot_general x1, matrix products, fold_accepted(): jnp.einsum('sph,sphd,sphv->shdv', weights, key_rows, value_rows, precisio...  7.96 us
    all_to_all x1, starting transfers between devices, shards(): lax.all_to_all(jnp.stack(jnp.split(normed, lax.axis_size('kv'), axis=1)),...  7.11 us
    unnamed x1, waiting for transfers between devices  6.65 us
    dot_general x1, matrix products, readout_block(): jnp.einsum('sthd,shdv->sthv', query_rows, base_mem, precision=highest)  4.24 us
  transfers between devices with their start and end apart: 2, of which 1 were waited for; matrix products, arithmetic and copies ran while one was open for 11% of the time, Pallas kernels for 0%

profile of v1, /device:TPU:16, one launch (start us, length us, event | category | flops | bytes accessed | tf_op | source)
XLA Modules:
  0.0 152.0 jit_solution(486488416204563328)
XLA Ops:
  0.6 1.0 reshape.103
  1.6 1.9 %all_gather.3 = bf16[30,2048]{1,0:T(8,128)(2,1)S(1)} all-gather(bf16[30,1024]{1,0:T(8,128)(2,1)S(1)} %reshape.103), channel_id=1, replica_groups=mesh['kv'=16,'tp'=2] {'tp'}, dimensions={1}, use_global_device_ids=true | all-gather | bytes 184320 | tf_op jit(solution)/shard_map/all_gather | solution.py:83
  3.7 0.8 fusion.15
  4.5 0.6 constant_dynamic-update-slice_fusion.15
  6.3 0.6 constant_dynamic-update-slice_fusion.12
  6.9 0.6 constant_dynamic-update-slice_fusion.11
  7.5 0.6 constant_dynamic-update-slice_fusion.10
  8.1 0.6 constant_dynamic-update-slice_fusion.9
  8.7 0.6 constant_dynamic-update-slice_fusion.8
  9.3 0.6 constant_dynamic-update-slice_fusion.7
  9.8 0.6 constant_dynamic-update-slice_fusion.6
  10.4 0.6 constant_dynamic-update-slice_fusion.5
  11.6 0.6 constant_dynamic-update-slice_fusion.3
  12.2 0.6 constant_dynamic-update-slice_fusion.2
  12.8 0.6 constant_dynamic-update-slice_fusion.1
  14.0 7.1 %all-to-all-start = ((bf16[16,30,128]{2,1,0:T(8,128)(2,1)}), bf16[16,30,128]{2,1,0:T(8,128)(2,1)S(1)}, u32[]{:S(2)}, u32[]{:S(2)}) async-start(bf16[16,30,128]{2,1,0:T(8,128)(2,1)} %constant_dynamic-update-slice_fusion), calls=%async_computation | async-start | bytes 262144 | tf_op jit(solution)/shard_map/all_to_all | solution.py:92
  21.2 0.7 iota_compare_fusion
  21.8 0.7 dynamic_slice.15
  22.6 0.7 dynamic_slice.13
  23.3 0.7 fusion.31
  24.1 0.7 fusion.44
  24.9 0.8 copy.117
  25.8 0.8 reshape.112
  26.6 0.9 fusion.37
  27.8 0.9 convolution_add_fusion
  29.4 8.0 %multiply_add_fusion = f32[10,4,128,256]{3,2,1,0:T(8,128)} fusion(f32[10,4,128,256]{3,2,1,0:T(8,128)} %param.31, f32[10,4]{1,0:T(8,128)S(1)} %get-tuple-element.14, bf16[10,3,4,256]{3,1,2,0:T(4,128)(2,1)S(1)} %bitcast.117, f32[10,3,4,128]{3,2,1,0:T(4,128)S(1)} %get-tuple-element.19), kind=kOutput, calls=%fused_computation | convolution fusion | flops 49807360 | bytes 10608800 | tf_op jit(solution)/shard_map/sph,sphd,sphv->shdv/dot_general | solution.py:22
  39.4 2.5 %fusion.7 = f32[480,2048]{1,0:T(8,128)} fusion(bf16[480,128]{1,0:T(8,128)(2,1)S(1)} %reshape.104, bf16[128,1024]{1,0:T(8,128)(2,1)S(1)} %copy-done.1, bf16[128,512]{1,0:T(8,128)(2,1)S(1)} %copy-done.2, bf16[128,512]{1,0:T(8,128)(2,1)S(1)} %copy-done.3), kind=kOutput, calls=%fused_computation.12 | convolution fusion | flops 253231104 | bytes 4579328 | tf_op jit(solution)/shard_map/dot_general | solution.py:96
  41.9 94.6 %fusion = f32[32,2048]{1,0:T(8,128)S(1)} fusion(f32[480,2048]{1,0:T(8,128)} %fusion.7), kind=kCustom, calls=%all-reduce-scatter | all-reduce-scatter fusion | flops 1048577 | bytes 4194816
  136.6 1.9 %collective-permute-start = (bf16[30,2048]{1,0:T(8,128)(2,1)S(1)}, bf16[30,2048]{1,0:T(8,128)(2,1)S(1)}, u32[]{:S(2)}, u32[]{:S(2)}) collective-permute-start(bf16[30,2048]{1,0:T(8,128)(2,1)S(1)} %slice.23), channel_id=1, source_target_pairs={{0,2},{2,4},{4,6},{6,8},{8,10},{10,12},{12,14},{14,16},{16,18},{18... | collective-permute-start | bytes 368648
  138.6 6.6 %collective-permute-done = bf16[30,2048]{1,0:T(8,128)(2,1)S(1)} collective-permute-done((bf16[30,2048]{1,0:T(8,128)(2,1)S(1)}, bf16[30,2048]{1,0:T(8,128)(2,1)S(1)}, u32[]{:S(2)}, u32[]{:S(2)}) %collective-permute-start) | collective-permute-done | bytes 122912
  146.8 4.2 %fusion.3 = f32[10,3,4,256]{3,1,2,0:T(4,128)S(1)} fusion(f32[10,4,128,256]{3,2,1,0:T(8,128)} %multiply_add_fusion, f32[10,3,4]{1,2,0:T(4,128)S(1)} %copy.124, bf16[10,3,4,128]{3,2,1,0:T(4,128)(2,1)S(1)} %reshape.106), kind=kOutput, calls=%fused_computation.5 | convolution fusion | flops 47216640 | bytes 5396960 | tf_op jit(solution)/shard_map/sthd,shdv->sthv/dot_general | solution.py:49
  151.0 1.0 fusion.4
  (62 shorter events, 6.6 us)
Async XLA Ops:
  0.6 28.8 %copy-start = (bf16[10,3,1024]{2,1,0:T(4,128)(2,1)S(1)}, bf16[10,3,1024]{2,1,0:T(4,128)(2,1)}, u32[]{:S(2)}) copy-start(bf16[10,3,1024]{2,1,0:T(4,128)(2,1)} %param.27) | copy-start | bytes 184324
  14.0 25.2 %all-to-all-start = ((bf16[16,30,128]{2,1,0:T(8,128)(2,1)}), bf16[16,30,128]{2,1,0:T(8,128)(2,1)S(1)}, u32[]{:S(2)}, u32[]{:S(2)}) async-start(bf16[16,30,128]{2,1,0:T(8,128)(2,1)} %constant_dynamic-update-slice_fusion), calls=%async_computation | async-start | bytes 262144 | tf_op jit(solution)/shard_map/all_to_all | solution.py:92
  25.8 120.8 %copy-start.6 = (f32[10,4]{0,1:T(4,128)}, f32[10,4]{0,1:T(4,128)S(1)}, u32[]{:S(2)}) copy-start(f32[10,4]{0,1:T(4,128)S(1)} %copy.119) | copy-start | bytes 484
  29.4 8.2 %copy-start.7 = (u32[32]{0:T(128)S(1)}, u32[32]{0:T(128)}, u32[]{:S(2)}) copy-start(u32[32]{0:T(128)} %constant.39) | copy-start | bytes 388
  29.4 9.9 %copy-start.1 = (bf16[128,1024]{1,0:T(8,128)(2,1)S(1)}, bf16[128,1024]{1,0:T(8,128)(2,1)}, u32[]{:S(2)}) copy-start(bf16[128,1024]{1,0:T(8,128)(2,1)} %param.21) | copy-start | bytes 786436
  29.4 9.9 %copy-start.2 = (bf16[128,512]{1,0:T(8,128)(2,1)S(1)}, bf16[128,512]{1,0:T(8,128)(2,1)}, u32[]{:S(2)}) copy-start(bf16[128,512]{1,0:T(8,128)(2,1)} %param.20) | copy-start | bytes 393220
  29.4 9.9 %copy-start.3 = (bf16[128,512]{1,0:T(8,128)(2,1)S(1)}, bf16[128,512]{1,0:T(8,128)(2,1)}, u32[]{:S(2)}) copy-start(bf16[128,512]{1,0:T(8,128)(2,1)} %param.19) | copy-start | bytes 393220
  39.4 99.2 %copy-start.4 = (f32[10,4,128]{2,1,0:T(4,128)S(1)}, f32[10,4,128]{2,1,0:T(4,128)}, u32[]{:S(2)}) copy-start(f32[10,4,128]{2,1,0:T(4,128)} %param.32) | copy-start | bytes 61444
  136.6 8.7 %collective-permute-start = (bf16[30,2048]{1,0:T(8,128)(2,1)S(1)}, bf16[30,2048]{1,0:T(8,128)(2,1)S(1)}, u32[]{:S(2)}, u32[]{:S(2)}) collective-permute-start(bf16[30,2048]{1,0:T(8,128)(2,1)S(1)} %slice.23), channel_id=1, source_target_pairs={{0,2},{2,4},{4,6},{6,8},{8,10},{10,12},{12,14},{14,16},{16,18},{18... | collective-permute-start | bytes 368648
  138.6 13.4 %copy-start.5 = (f32[10,4,128]{2,1,0:T(4,128)}, f32[10,4,128]{2,1,0:T(4,128)S(1)}, u32[]{:S(2)}) copy-start(f32[10,4,128]{2,1,0:T(4,128)S(1)} %multiply_add_fusion.1) | copy-start | bytes 61444
